TPU v7x, 32 devices: a whole 2x2x4 slice. The times are simulated.
32 devices in a mesh: gr: 2 (over y), sp: 4 (over z), tp: 4 (over x, core).
Axes of the slice: x: 2, y: 2, z: 4, core: 2. Of those that a mesh axis runs over, the one named last changes fastest.
Arguments:
- tokens: bfloat16 [4, 1024, 4096], P('gr', ('sp', 'tp')), parts along dimension 0, may hold values from -6 to 6
- norm_gain: bfloat16 [4096], replicated, may hold values from 0.099609375 to 1.8984375
- key_weight: bfloat16 [4096, 1024], P(None, 'tp'), may hold values from -0.09375 to 0.09375
- value_weight: bfloat16 [4096, 1024], P(None, 'tp'), may hold values from -0.09375 to 0.09375
- cum_gates: float32 [4, 1024, 16], P('gr', 'sp', 'tp'), parts along dimension 0, may hold values from -173 to 0, as said below
- new_query: bfloat16 [4, 1024], P('gr', 'tp'), parts along dimension 0, may hold values from -240 to 240
- new_key: bfloat16 [4, 1024], P('gr', 'tp'), parts along dimension 0, may hold values from -6 to 6
- new_value: bfloat16 [4, 1024], P('gr', 'tp'), parts along dimension 0, may hold values from -6 to 6
- new_gate: float32 [4, 16], P('gr', 'tp'), parts along dimension 0, may hold values from -5 to -1.5
Outputs:
- key_cache: bfloat16 [4, 1024, 1024], P('gr', 'sp', 'tp'), parts along dimension 0
- value_cache: bfloat16 [4, 1024, 1024], P('gr', 'sp', 'tp'), parts along dimension 0
- readout: bfloat16 [4, 1024], P('gr', 'tp'), parts along dimension 0
There are 2 independent parts, one for each index of `gr`. A program takes and returns all parts, laid end to end along the dimension named above; an argument that names none is the same for every part. Nothing has to cross between parts.
Inputs may be any that keep to these rules, and one draw needn't show every extreme that they name: `cum_gates`: along positions, for each prompt and head, the values never rise.
All inputs are finite; a program needn't handle non-finite values.
Results may differ from a plain program's by a relative error of at most 0.005.
The roundings to bfloat16 on the way count: a program that leaves them out, or rounds other values in their place, can miss the bound.
Values may be sent and summed in bfloat16 or wider, within the bound.
A program may use at most 64 MiB of HBM per device.

v0:
```python
import jax
import jax.numpy as jnp
from jax import lax
from jax.sharding import PartitionSpec as P

HD = 64
epsilon = 1e-06
masked_score = -1e30


def body(
    tokens, norm_gain, key_weight, value_weight, cum_gates, new_query, new_key, new_value, new_gate
):
    seq_count, own_len, model_width = tokens.shape
    as_float = tokens.astype(jnp.float32)
    normed = (
        as_float
        * lax.rsqrt(jnp.mean(as_float * as_float, axis=-1, keepdims=True) + epsilon)
        * norm_gain.astype(jnp.float32)
    ).astype(jnp.bfloat16)
    key_width = key_weight.shape[1]
    local_heads = key_width // HD
    both_weights = jnp.concatenate([key_weight, value_weight], axis=1)
    piece = lax.all_gather(normed, "tp", axis=1, tiled=True)
    piece_len = piece.shape[1]
    rows = piece.reshape(seq_count * piece_len, model_width)
    result = jnp.dot(rows, both_weights, preferred_element_type=jnp.float32).astype(jnp.bfloat16)
    projected = result.reshape(seq_count, piece_len, 2 * key_width)
    key_cache = projected[:, :, :key_width]
    value_cache = projected[:, :, key_width:]
    block_len = projected.shape[1]
    sp_count = lax.axis_size("sp")
    sp_index = lax.axis_index("sp")
    score_scale = HD ** (-0.5)
    queries = new_query.reshape(seq_count, local_heads, HD)
    fresh_key = new_key.reshape(seq_count, local_heads, HD).astype(jnp.float32)
    fresh_value = new_value.reshape(seq_count, local_heads, HD).astype(jnp.float32)
    fresh_score = jnp.sum(queries.astype(jnp.float32) * fresh_key, axis=-1) * score_scale
    key_heads = key_cache.reshape(seq_count, block_len, local_heads, HD)
    value_heads = value_cache.reshape(seq_count, block_len, local_heads, HD).astype(jnp.float32)
    scores = (
        jnp.einsum("shd,slhd->shl", queries, key_heads, preferred_element_type=jnp.float32)
        * score_scale
    )
    scores = scores - jnp.transpose(cum_gates, (0, 2, 1))
    last_block = sp_index == sp_count - 1
    fresh_term = jnp.where(
        last_block, fresh_score - (cum_gates[:, block_len - 1, :] + new_gate), masked_score
    )
    local_top = jnp.maximum(jnp.max(scores, axis=-1), fresh_term)
    maxima = lax.pmax(local_top, "sp")
    weights = jnp.exp(scores - maxima[:, :, None])
    fresh_weight = jnp.exp(fresh_term - maxima)
    totals = jnp.sum(weights, axis=-1) + fresh_weight
    weighted = jnp.einsum("shl,slhd->shd", weights, value_heads, precision=lax.Precision.HIGHEST)
    weighted = weighted + fresh_weight[:, :, None] * fresh_value
    totals, weighted = lax.psum((totals, weighted), "sp")
    readout = (weighted / totals[:, :, None]).reshape(seq_count, key_width).astype(jnp.bfloat16)
    return (key_cache, value_cache, readout)


def solution(mesh):
    in_specs = (
        P("gr", ("sp", "tp"), None),
        P(),
        P(None, "tp"),
        P(None, "tp"),
        P("gr", "sp", "tp"),
        P("gr", "tp"),
        P("gr", "tp"),
        P("gr", "tp"),
        P("gr", "tp"),
    )
    out_specs = (P("gr", "sp", "tp"), P("gr", "sp", "tp"), P("gr", "tp"))
    return jax.shard_map(body, mesh=mesh, in_specs=in_specs, out_specs=out_specs, check_vma=False)
```

profile of v0, /device:TPU:0, one launch (start us, length us, event | category | flops | bytes accessed | tf_op | source)
XLA Modules:
  0.0 83.7 jit_solution(6548077247722289311)
XLA Ops:
  7.2 0.0 all-gather.2.cloned.1.call-start
  7.2 0.7 convert_element_type.35
  7.9 0.0 copy-start.3
  7.9 0.0 copy-start.4
  7.9 0.0 copy-start.5
  7.9 0.0 copy-start.2
  7.9 0.0 copy-start.7
  7.9 1.7 %fusion.4 = f32[2,64]{1,0:T(2,128)S(1)} fusion(bf16[2,64,4096]{2,1,0:T(8,128)(2,1)} %param.9), kind=kLoop, calls=%fused_computation.6 | loop fusion | flops 1572736 | bytes 1049088 | tf_op jit(solution)/shard_map/reduce_sum | solution.py:18
  9.6 2.5 %fusion.6 = bf16[2,64,4096]{2,1,0:T(8,128)(2,1)} fusion(bf16[2,64,4096]{2,1,0:T(8,128)(2,1)} %param.9, f32[4096]{0:T(1024)S(1)} %convert_element_type.35, f32[2,64]{1,0:T(2,128)S(1)} %add_rsqrt_fusion), kind=kLoop, calls=%fused_computation.8 | loop fusion | flops 2097152 | bytes 2114048 | tf_op jit(solution)/shard_map/convert_element_type | solution.py:20
  12.2 0.0 all-gather.2.cloned.1.call-update
  12.2 0.0 copy-done.3
  12.2 0.1 reshape.53
  12.3 0.1 reshape.44
  12.4 0.0 copy-done.4
  12.4 0.1 reshape.46
  12.4 0.0 copy-done.5
  12.4 0.1 reshape.47
  12.5 0.0 copy-done.2
  12.5 0.2 slice_reduce_fusion
  12.7 0.1 multiply_reduce_fusion
  12.8 36.7 %all-gather.2.cloned.1.call-done = bf16[2,256,4096]{2,1,0:T(8,128)(2,1)} async-done(((bf16[2,64,4096]{2,1,0:T(8,128)(2,1)}), bf16[2,256,4096]{2,1,0:T(8,128)(2,1)}) %all-gather.2.cloned.1.call-update) | async-done | bytes 4194320 | tf_op jit(solution)/shard_map/all_gather | solution.py:24
  49.5 0.0 copy-done.7
  49.5 0.0 copy-start.6
  49.5 5.2 %fusion.7 = bf16[512,512]{1,0:T(8,128)(2,1)S(1)} fusion(bf16[512,4096]{1,0:T(8,128)(2,1)} %bitcast.34, bf16[4096,256]{1,0:T(8,128)(2,1)S(1)} %copy-done.7, bf16[4096,256]{1,0:T(8,128)(2,1)} %param.11), kind=kOutput, calls=%fused_computation.9 | convolution fusion | flops 2156134400 | bytes 8912896 | tf_op jit(solution)/shard_map/dot_general | solution.py:27
  54.8 0.0 copy-start
  54.8 0.0 copy-start.1
  54.8 0.1 copy.20
  55.0 0.1 fusion.19
  55.1 0.1 fusion.15
  55.2 0.0 copy-done.6
  55.2 11.7 %pmax.7 = f32[2,4]{1,0:T(2,128)S(1)} all-reduce(f32[2,4]{1,0:T(2,128)S(1)} %get-tuple-element.10), channel_id=1, replica_groups=mesh['gr'=2,'sp'=4,'tp'=4] {'sp'}, use_global_device_ids=true, to_apply=%region_3.4 | all-reduce | flops 8 | bytes 64 | tf_op jit(solution)/shard_map/pmax | solution.py:51
  66.9 0.2 fusion.12
  67.1 0.1 copy.21
  67.2 0.3 fusion.10
  67.5 0.1 multiply_add_fusion
  67.6 8.5 %all-reduce = (f32[2,4,64]{2,1,0:T(4,128)S(1)}, f32[2,4]{1,0:T(2,128)S(1)}) all-reduce(f32[2,4,64]{2,1,0:T(4,128)S(1)} %multiply_add_fusion, f32[2,4]{1,0:T(2,128)S(1)} %get-tuple-element.8), channel_id=1, replica_groups=mesh['gr'=2,'sp'=4,'tp'=4] {'sp'}, use_global_device_ids=true, to_apply=%region_4.5 | all-reduce | flops 520 | bytes 4160 | tf_op jit(solution)/shard_map/psum | solution.py:57
  76.1 0.1 divide_convert_fusion
  76.2 0.7 convert_element_type.44
  76.9 0.0 copy-done
  76.9 0.0 copy-done.1
  (4 shorter events, 0.1 us)
Async XLA Ops:
  7.2 42.3 %all-gather.2.cloned.1.call-start = ((), (), s32[]{:S(2)}) async-start(), calls=%async_computation | async-start | bytes 5242880 | tf_op jit(solution)/shard_map/all_gather | solution.py:24
  7.9 4.3 %copy-start.3 = (bf16[2,256]{1,0:T(2,128)(2,1)S(1)}, bf16[2,256]{1,0:T(2,128)(2,1)}, u32[]{:S(2)}) copy-start(bf16[2,256]{1,0:T(2,128)(2,1)} %param.14) | copy-start | bytes 3076
  7.9 4.4 %copy-start.4 = (bf16[2,256]{1,0:T(2,128)(2,1)S(1)}, bf16[2,256]{1,0:T(2,128)(2,1)}, u32[]{:S(2)}) copy-start(bf16[2,256]{1,0:T(2,128)(2,1)} %param.15) | copy-start | bytes 3076
  7.9 4.5 %copy-start.5 = (bf16[2,256]{1,0:T(2,128)(2,1)S(1)}, bf16[2,256]{1,0:T(2,128)(2,1)}, u32[]{:S(2)}) copy-start(bf16[2,256]{1,0:T(2,128)(2,1)} %param.16) | copy-start | bytes 3076
  7.9 4.6 %copy-start.2 = (f32[2,256,4]{1,2,0:T(4,128)S(1)}, f32[2,256,4]{1,2,0:T(4,128)}, u32[]{:S(2)}) copy-start(f32[2,256,4]{1,2,0:T(4,128)} %param.13) | copy-start | bytes 24580
  7.9 41.6 %copy-start.7 = (bf16[4096,256]{1,0:T(8,128)(2,1)S(1)}, bf16[4096,256]{1,0:T(8,128)(2,1)}, u32[]{:S(2)}) copy-start(bf16[4096,256]{1,0:T(8,128)(2,1)} %param.12) | copy-start | bytes 6291460
  49.5 5.7 %copy-start.6 = (f32[2,4]{1,0:T(2,128)S(1)}, f32[2,4]{1,0:T(2,128)}, u32[]{:S(2)}) copy-start(f32[2,4]{1,0:T(2,128)} %param.17) | copy-start | bytes 100
  54.8 22.1 %copy-start = (bf16[2,256,256]{2,1,0:T(8,128)(2,1)}, bf16[2,256,256]{2,1,0:T(8,128)(2,1)S(1)}, u32[]{:S(2)}) copy-start(bf16[2,256,256]{2,1,0:T(8,128)(2,1)S(1)} %get-tuple-element.12) | copy-start | bytes 786436
  54.8 22.0 %copy-start.1 = (bf16[2,256,256]{2,1,0:T(8,128)(2,1)}, bf16[2,256,256]{2,1,0:T(8,128)(2,1)S(1)}, u32[]{:S(2)}) copy-start(bf16[2,256,256]{2,1,0:T(8,128)(2,1)S(1)} %get-tuple-element.13) | copy-start | bytes 786436
Sparse Core Ops, SparseCore 0:
  12.3 37.1 all-gather.1
where the time goes:
time: 84 us; the launch traced here: 83.7 us
  waiting for transfers between devices  36.8 us (44%)
  blocking collectives  20.2 us (24%)
  between operations  14.1 us (17%)
  matrix products  5.69 us (7%)
  other arithmetic  5.42 us (6%)
  local copies, waits for them, and re-layouts  1.48 us (2%)
    all_gather x1, waiting for transfers between devices, body(): piece = lax.all_gather(normed, 'tp', axis=1, tiled=True)  36.7 us
    pmax x1, blocking collectives, body(): maxima = lax.pmax(local_top, 'sp')  11.7 us
    psum x1, blocking collectives, body(): totals, weighted = lax.psum((totals, weighted), 'sp')  8.5 us
    dot_general x1, matrix products, body(): jnp.dot(rows, both_weights, preferred_element_type=jnp.float32)  5.24 us
    convert_element_type x1, other arithmetic, body(): normed = (as_float * lax.rsqrt(jnp.mean(as_float * as_float, axis=-1, kee...  2.53 us
  transfers between devices with their start and end apart: 1, of which 1 were waited for; matrix products, arithmetic and copies ran while one was open for 1% of the time, Pallas kernels for 0%

commit v1 on v0

--- a/solution.py
+++ b/solution.py
@@ -6,6 +6,17 @@
 HD = 64
 epsilon = 1e-06
 masked_score = -1e30
+
+
+def pass_along(array, mesh_axis, dim):
+    size = lax.axis_size(mesh_axis)
+    hops = [(i, (i + 1) % size) for i in range(size)]
+    parts = [array]
+    for far in range(1, size):
+        parts = [lax.ppermute(parts[0], mesh_axis, hops), *parts]
+    whole = jnp.concatenate(parts, axis=dim)
+    shift = (lax.axis_index(mesh_axis) + 1) * parts[-1].shape[dim]
+    return jnp.roll(whole, shift, axis=dim)
 
 
 def body(
@@ -21,7 +32,7 @@
     key_width = key_weight.shape[1]
     local_heads = key_width // HD
     both_weights = jnp.concatenate([key_weight, value_weight], axis=1)
-    piece = lax.all_gather(normed, "tp", axis=1, tiled=True)
+    piece = pass_along(normed, "tp", 1)
     piece_len = piece.shape[1]
     rows = piece.reshape(seq_count * piece_len, model_width)
     result = jnp.dot(rows, both_weights, preferred_element_type=jnp.float32).astype(jnp.bfloat16)

time: 84 us -> 79.8 us (0.950)
  between operations: 14.1 us -> 0.8 us
  local copies, waits for them, and re-layouts: 1.48 us -> 9.94 us
  matrix products: 5.69 us -> 2.8 us
  waiting for transfers between devices: 36.8 us -> 39 us
  blocking collectives: 20.2 us -> 21.3 us
    ppermute x0 -> x3, waiting for transfers between devices: none -> 39 us  [pass_along(): parts = [lax.ppermute(parts[0], mesh_axis, hops), *parts]]
    all_gather x1 -> x0, waiting for transfers between devices: 36.7 us -> none  [body(): piece = lax.all_gather(normed, 'tp', axis=1, tiled=True)]
    unnamed x18 -> x22, local copies, waits for them, and re-layouts: 0.3 us -> 4.87 us
    dot_general x1, matrix products: 5.24 us -> 2.35 us  [body(): jnp.dot(rows, both_weights, preferred_element_type=jnp.float32)]
    reshape x2, local copies, waits for them, and re-layouts: 0.17 us -> 1.52 us  [body(): queries = new_query.reshape(seq_count, local_heads, HD)]
    pmax x1, blocking collectives: 11.7 us -> 12.8 us  [body(): maxima = lax.pmax(local_top, 'sp')]
    convert_element_type x1, other arithmetic: 2.53 us -> 1.64 us  [body(): normed = (as_float * lax.rsqrt(jnp.mean(as_float * as_float, axis=-1, kee...]
  transfers between devices with their start and end apart: 1 -> 3, of which waited for: 1 -> 3; matrix products, arithmetic and copies ran while one was open for 1% -> 5% of each run, Pallas kernels for 0% -> 0%
where the time goes in v1:
time: 79.8 us; the launch traced here: 79.3 us
  waiting for transfers between devices  39 us (49%)
  blocking collectives  21.3 us (27%)
  local copies, waits for them, and re-layouts  9.94 us (12%)
  other arithmetic  5.01 us (6%)
  matrix products  2.8 us (4%)
  between operations  0.8 us (1%)
    ppermute x3, waiting for transfers between devices, pass_along(): parts = [lax.ppermute(parts[0], mesh_axis, hops), *parts]  39 us
    pmax x1, blocking collectives, body(): maxima = lax.pmax(local_top, 'sp')  12.8 us
    psum x1, blocking collectives, body(): totals, weighted = lax.psum((totals, weighted), 'sp')  8.5 us
    unnamed x22, local copies, waits for them, and re-layouts  4.87 us
    dot_general x1, matrix products, body(): jnp.dot(rows, both_weights, preferred_element_type=jnp.float32)  2.35 us
    convert_element_type x1, other arithmetic, body(): normed = (as_float * lax.rsqrt(jnp.mean(as_float * as_float, axis=-1, kee...  1.64 us
  transfers between devices with their start and end apart: 3, of which 3 were waited for; matrix products, arithmetic and copies ran while one was open for 5% of the time, Pallas kernels for 0%

profile of v1, /device:TPU:0, one launch (start us, length us, event | category | flops | bytes accessed | tf_op | source)
XLA Modules:
  0.0 79.3 jit_solution(12259363461523371212)
XLA Ops:
  0.6 0.7 convert_element_type.35
  1.3 1.5 %fusion.4 = f32[2,64]{1,0:T(2,128)S(1)} fusion(bf16[2,64,4096]{2,1,0:T(8,128)(2,1)} %param.9), kind=kLoop, calls=%fused_computation.6 | loop fusion | flops 1572736 | bytes 1049088 | tf_op jit(solution)/shard_map/reduce_sum | solution.py:29
  2.9 0.0 copy-start
  2.9 1.6 %fusion.6 = bf16[2,64,4096]{2,1,0:T(8,128)(2,1)S(1)} fusion(bf16[2,64,4096]{2,1,0:T(8,128)(2,1)} %param.9, f32[4096]{0:T(1024)S(1)} %convert_element_type.35, f32[2,64]{1,0:T(2,128)S(1)} %add_rsqrt_fusion), kind=kLoop, calls=%fused_computation.8 | loop fusion | flops 2097152 | bytes 2114048 | tf_op jit(solution)/shard_map/convert_element_type | solution.py:31
  4.5 0.5 collective-permute-start
  5.1 14.4 %collective-permute-done = bf16[2,64,4096]{2,1,0:T(8,128)(2,1)S(1)} collective-permute-done((bf16[2,64,4096]{2,1,0:T(8,128)(2,1)S(1)}, bf16[2,64,4096]{2,1,0:T(8,128)(2,1)S(1)}, u32[]{:S(2)}, u32[]{:S(2)}) %collective-permute-start) | collective-permute-done | bytes 1048608 | tf_op jit(solution)/shard_map/ppermute | solution.py:16
  19.5 0.0 collective-permute-start.1
  19.5 14.2 %collective-permute-done.1 = bf16[2,64,4096]{2,1,0:T(8,128)(2,1)S(1)} collective-permute-done((bf16[2,64,4096]{2,1,0:T(8,128)(2,1)S(1)}, bf16[2,64,4096]{2,1,0:T(8,128)(2,1)S(1)}, u32[]{:S(2)}, u32[]{:S(2)}) %collective-permute-start.1) | collective-permute-done | bytes 1048608 | tf_op jit(solution)/shard_map/ppermute | solution.py:16
  33.7 0.0 collective-permute-start.2
  33.7 0.8 reshape.53
  34.4 0.8 reshape.44
  35.2 0.8 reshape.46
  36.0 0.8 reshape.47
  36.7 0.8 %slice_reduce_fusion = f32[2,4]{1,0:T(2,128)S(1)} fusion(f32[2,256,4]{1,2,0:T(4,128)} %param.13), kind=kLoop, calls=%fused_computation.26 | loop fusion | bytes 64 | tf_op jit(solution)/shard_map/slice | solution.py:59
  37.6 0.1 multiply_reduce_fusion
  37.7 10.4 %collective-permute-done.2 = bf16[2,64,4096]{2,1,0:T(8,128)(2,1)} collective-permute-done((bf16[2,64,4096]{2,1,0:T(8,128)(2,1)S(1)}, bf16[2,64,4096]{2,1,0:T(8,128)(2,1)}, u32[]{:S(2)}, u32[]{:S(2)}) %collective-permute-start.2) | collective-permute-done | bytes 1048608 | tf_op jit(solution)/shard_map/ppermute | solution.py:16
  48.0 1.3 %constant_dynamic-update-slice_fusion.7 = bf16[2,512,4096]{2,1,0:T(8,128)(2,1)S(1)} fusion(bf16[2,64,4096]{2,1,0:T(8,128)(2,1)} %collective-permute-done.2), kind=kLoop, calls=%fused_computation.17 | loop fusion | bytes 2097152
  49.3 0.1 constant_dynamic-update-slice_fusion.6
  49.4 0.1 constant_dynamic-update-slice_fusion.5
  49.5 0.0 copy-done
  49.5 0.3 constant_dynamic-update-slice_fusion.4
  49.8 1.3 %constant_dynamic-update-slice_fusion.3 = bf16[2,512,4096]{2,1,0:T(8,128)(2,1)S(1)} fusion(bf16[2,512,4096]{2,1,0:T(8,128)(2,1)S(1)} %constant_dynamic-update-slice_fusion.4, bf16[2,64,4096]{2,1,0:T(8,128)(2,1)} %collective-permute-done.2), kind=kLoop, calls=%fused_computation.13 | loop fusion | bytes 2097152
  51.1 0.1 constant_dynamic-update-slice_fusion.2
  51.2 0.1 constant_dynamic-update-slice_fusion.1
  51.3 0.3 constant_dynamic-update-slice_fusion
  51.6 0.0 copy-start.5
  51.6 0.0 copy-start.6
  51.6 0.5 constant_dynamic-slice_fusion
  52.1 1.1 %copy-done.5 = bf16[4096,256]{1,0:T(8,128)(2,1)S(1)} copy-done((bf16[4096,256]{1,0:T(8,128)(2,1)S(1)}, bf16[4096,256]{1,0:T(8,128)(2,1)}, u32[]{:S(2)}) %copy-start.5) | copy-done | bytes 2097176
  53.2 0.6 copy-done.6
  53.8 0.0 copy-start.3
  53.8 0.0 copy-start.4
  53.8 2.3 %fusion.7 = bf16[512,512]{1,0:T(8,128)(2,1)S(1)} fusion(bf16[512,4096]{1,0:T(8,128)(2,1)S(1)} %bitcast.30, bf16[4096,256]{1,0:T(8,128)(2,1)S(1)} %copy-done.5, bf16[4096,256]{1,0:T(8,128)(2,1)S(1)} %copy-done.6), kind=kOutput, calls=%fused_computation.9 | convolution fusion | flops 2156134400 | bytes 8912896 | tf_op jit(solution)/shard_map/dot_general | solution.py:38
  56.2 0.0 copy-start.1
  56.2 0.0 copy-start.2
  56.2 0.1 copy.21
  56.4 0.1 copy.20
  56.5 0.1 fusion.19
  56.7 0.0 copy-done.3
  56.7 0.1 fusion.15
  56.8 0.0 copy-done.4
  56.8 12.8 %pmax.7 = f32[2,4]{1,0:T(2,128)S(1)} all-reduce(f32[2,4]{1,0:T(2,128)S(1)} %get-tuple-element.10), channel_id=1, replica_groups=mesh['gr'=2,'sp'=4,'tp'=4] {'sp'}, use_global_device_ids=true, to_apply=%region_3.4 | all-reduce | flops 8 | bytes 64 | tf_op jit(solution)/shard_map/pmax | solution.py:62
  69.5 0.2 fusion.12
  69.7 0.3 fusion.10
  70.0 0.1 multiply_add_fusion
  70.1 8.5 %all-reduce = (f32[2,4,64]{2,1,0:T(4,128)S(1)}, f32[2,4]{1,0:T(2,128)S(1)}) all-reduce(f32[2,4,64]{2,1,0:T(4,128)S(1)} %multiply_add_fusion, f32[2,4]{1,0:T(2,128)S(1)} %get-tuple-element.8), channel_id=1, replica_groups=mesh['gr'=2,'sp'=4,'tp'=4] {'sp'}, use_global_device_ids=true, to_apply=%region_4.5 | all-reduce | flops 520 | bytes 4160 | tf_op jit(solution)/shard_map/psum | solution.py:68
  78.6 0.1 divide_convert_fusion
  78.7 0.7 convert_element_type.44
  79.3 0.0 copy-done.1
  79.3 0.0 copy-done.2
  (4 shorter events, 0.1 us)
Async XLA Ops:
  2.9 46.6 %copy-start = (bf16[2,64,4096]{2,1,0:T(8,128)(2,1)S(1)}, bf16[2,64,4096]{2,1,0:T(8,128)(2,1)}, u32[]{:S(2)}) copy-start(bf16[2,64,4096]{2,1,0:T(8,128)(2,1)} %param.9) | copy-start | bytes 3145732
  4.5 14.9 %collective-permute-start = (bf16[2,64,4096]{2,1,0:T(8,128)(2,1)S(1)}, bf16[2,64,4096]{2,1,0:T(8,128)(2,1)S(1)}, u32[]{:S(2)}, u32[]{:S(2)}) collective-permute-start(bf16[2,64,4096]{2,1,0:T(8,128)(2,1)S(1)} %fusion.6), channel_id=1, source_target_pairs={{0,1},{1,2},{2,3},{3,0},{4,5},{5,6},{6,7},{7,4},{8,9},{9,10},{10,1... | collective-permute-start | bytes 3145736 | tf_op jit(solution)/shard_map/ppermute | solution.py:16
  19.5 14.2 %collective-permute-start.1 = (bf16[2,64,4096]{2,1,0:T(8,128)(2,1)S(1)}, bf16[2,64,4096]{2,1,0:T(8,128)(2,1)S(1)}, u32[]{:S(2)}, u32[]{:S(2)}) collective-permute-start(bf16[2,64,4096]{2,1,0:T(8,128)(2,1)S(1)} %collective-permute-done), channel_id=1, source_target_pairs={{0,1},{1,2},{2,3},{3,0},{4,5},{5,6},{6,7},{7,4},{8,9},{9,10},{10,1... | collective-permute-start | bytes 3145736 | tf_op jit(solution)/shard_map/ppermute | solution.py:16
  33.7 14.3 %collective-permute-start.2 = (bf16[2,64,4096]{2,1,0:T(8,128)(2,1)S(1)}, bf16[2,64,4096]{2,1,0:T(8,128)(2,1)}, u32[]{:S(2)}, u32[]{:S(2)}) collective-permute-start(bf16[2,64,4096]{2,1,0:T(8,128)(2,1)S(1)} %collective-permute-done.1), channel_id=1, source_target_pairs={{0,1},{1,2},{2,3},{3,0},{4,5},{5,6},{6,7},{7,4},{8,9},{9,10},{10,1... | collective-permute-start | bytes 3145736 | tf_op jit(solution)/shard_map/ppermute | solution.py:16
  51.6 1.6 %copy-start.5 = (bf16[4096,256]{1,0:T(8,128)(2,1)S(1)}, bf16[4096,256]{1,0:T(8,128)(2,1)}, u32[]{:S(2)}) copy-start(bf16[4096,256]{1,0:T(8,128)(2,1)} %param.12) | copy-start | bytes 6291460
  51.6 2.2 %copy-start.6 = (bf16[4096,256]{1,0:T(8,128)(2,1)S(1)}, bf16[4096,256]{1,0:T(8,128)(2,1)}, u32[]{:S(2)}) copy-start(bf16[4096,256]{1,0:T(8,128)(2,1)} %param.11) | copy-start | bytes 6291460
  53.8 2.9 %copy-start.3 = (f32[2,256,4]{1,2,0:T(4,128)S(1)}, f32[2,256,4]{1,2,0:T(4,128)}, u32[]{:S(2)}) copy-start(f32[2,256,4]{1,2,0:T(4,128)} %param.13) | copy-start | bytes 24580
  53.8 3.0 %copy-start.4 = (f32[2,4]{1,0:T(2,128)S(1)}, f32[2,4]{1,0:T(2,128)}, u32[]{:S(2)}) copy-start(f32[2,4]{1,0:T(2,128)} %param.17) | copy-start | bytes 100
  56.2 23.1 %copy-start.1 = (bf16[2,256,256]{2,1,0:T(8,128)(2,1)}, bf16[2,256,256]{2,1,0:T(8,128)(2,1)S(1)}, u32[]{:S(2)}) copy-start(bf16[2,256,256]{2,1,0:T(8,128)(2,1)S(1)} %get-tuple-element.12) | copy-start | bytes 786436
  56.2 23.1 %copy-start.2 = (bf16[2,256,256]{2,1,0:T(8,128)(2,1)}, bf16[2,256,256]{2,1,0:T(8,128)(2,1)S(1)}, u32[]{:S(2)}) copy-start(bf16[2,256,256]{2,1,0:T(8,128)(2,1)S(1)} %get-tuple-element.13) | copy-start | bytes 786436
